TPU v7x, 256 devices: a whole 4x4x8 slice. The times are simulated.
256 devices in a mesh: rep: 2 (over z_hi), fs: 16 (over z_lo, y), tp: 8 (over x, core).
Axes of the slice: x: 4, y: 4, z: 8 (z_hi: 2, z_lo: 4; z = z_hi * 4 + z_lo), core: 2. Of those that a mesh axis runs over, the one named last changes fastest.
Arguments:
- stream: bfloat16 [32, 1024, 2048], P(('rep', 'fs'), None, 'tp'), may hold values from -6 to 6
- norm_gain: float32 [2048], replicated, may hold values from 0.1 to 1.9
- w_in: float32 [2048, 512], P('fs', 'tp'), may hold values from -0.125 to 0.125
- s_in: float32 [512], P(('tp', 'fs')), may hold values from 0.1 to 1.9
- pool_w: bfloat16 [4, 128, 128], replicated, may hold values from -0.5 to 0.5
- w_out: float32 [512, 2048], P('fs', 'tp'), may hold values from -0.25 to 0.25
- s_out: float32 [2048], P(('tp', 'fs')), may hold values from 0.1 to 1.9
- ffn_gain: float32 [2048], replicated, may hold values from 0.1 to 1.9
- w_up: float32 [2048, 8192], P('fs', 'tp'), may hold values from -0.125 to 0.125
- s_up: float32 [8192], P(('tp', 'fs')), may hold values from 0.1 to 1.9
- w_down: float32 [8192, 2048], P('tp', 'fs'), may hold values from -0.0625 to 0.0625
- s_down: float32 [2048], P('fs'), may hold values from 0.1 to 1.9
Outputs:
- result: bfloat16 [32, 1024, 2048], P(('rep', 'fs'), None, 'tp')
All inputs are finite; a program needn't handle non-finite values.
Results may differ from a plain program's by a relative error of at most 0.012.
Values may be sent and summed in bfloat16 or wider, within the bound.
No kernel may reach another device: no remote copies, remote signals or barrier semaphores. Data moves between devices by JAX's collectives and lax.ppermute only.
A program may use at most 64 MiB of HBM per device.

v0:
```python
import jax
import jax.numpy as jnp
from jax import lax
from jax.sharding import Mesh
from jax.sharding import PartitionSpec as P

PW = 512
GROUP = 128
FS = ("fs_0", "fs_1")
REP_FS = ("rep", "fs_0", "fs_1")
TP_FS = ("tp", "fs_0", "fs_1")
epsilon = 0.25


def laid_out(parts, dim):
    parts = jnp.moveaxis(parts, 0, dim)
    lengths = parts.shape
    return parts.reshape(*lengths[:dim], lengths[dim] * lengths[dim + 1], *lengths[dim + 2 :])


def gather_packed(arrays, axis, dims):
    ravelled = jnp.concatenate([a.reshape(-1) for a in arrays])
    lines, at, finished = (lax.all_gather(ravelled, axis), 0, [])
    for a, dim in zip(arrays, dims):
        parts = lines[:, at : at + a.size].reshape(-1, *a.shape)
        finished.append(laid_out(parts, dim))
        at += a.size
    return tuple(finished)


def sent_to_all(array, axis):
    count = lax.axis_size(axis)
    return lax.all_to_all(
        jnp.broadcast_to(array[None], (count, *array.shape)), axis, 0, 0, tiled=True
    )


def collect(array, axis, dim):
    return laid_out(sent_to_all(array, axis), dim)


def stacked_from(array, axes, turns):
    parts = array
    for k in turns:
        parts = lax.all_gather(parts, axes[k])
    done = turns[::-1]
    back = [done.index(k) for k in range(len(axes))]
    parts = parts.transpose(*back, *range(len(axes), parts.ndim))
    return parts.reshape(-1, *array.shape)


def whole_of(array, axes, turns, dim):
    return laid_out(stacked_from(array, axes, turns), dim)


def cut_along(array, dim, count):
    lengths = array.shape
    parts = array.reshape(*lengths[:dim], count, lengths[dim] // count, *lengths[dim + 1 :])
    return jnp.moveaxis(parts, dim, 0)


def sent_and_summed(array, axis, dim):
    count = lax.axis_size(axis)
    parts = lax.all_to_all(cut_along(array, dim, count), axis, 0, 0, tiled=True)
    return jnp.sum(parts.astype(jnp.float32), axis=0)


def rms_rows(values, gain):
    floats = values.astype(jnp.float32)
    scale = lax.rsqrt(jnp.mean(floats * floats, axis=-1, keepdims=True) + epsilon)
    return (floats * scale * gain).astype(jnp.bfloat16)


def pool_local(pool_in, first):
    length, width = pool_in.shape
    positions = jnp.arange(length, dtype=jnp.int32)
    source = positions[None, :]
    target = positions[:, None]
    group_of = (first + jnp.arange(width, dtype=jnp.int32)) // GROUP
    means = jnp.zeros((length, width), jnp.float32)
    for level in range(4):
        half = 2**level
        band_ones = ((source >= target - half) & (source < target + half)).astype(jnp.bfloat16)
        counts = (jnp.minimum(positions + half, length) - jnp.maximum(positions - half, 0)).astype(
            jnp.float32
        )
        sums = jnp.dot(band_ones, pool_in, preferred_element_type=jnp.float32) / counts[:, None]
        means = jnp.where(group_of[None, :] == level, sums, means)
    return (means - pool_in.astype(jnp.float32)).astype(jnp.bfloat16)


def fold_rows(left, piece):
    return jnp.dot(left, piece, preferred_element_type=jnp.float32)


def on_device(
    stream, norm_gain, w_in, s_in, pool_w, w_out, s_out, ffn_gain, w_up, s_up, w_down, s_down
):
    tokens = stream[0]
    length = tokens.shape[0]
    scale_in, scale_out, scale_up, scale_down = gather_packed(
        (s_in, s_out, s_up, s_down), FS, (0, 0, 0, 0)
    )
    in_whole, out_whole = gather_packed(
        (w_in.astype(jnp.bfloat16), w_out.astype(jnp.bfloat16)), FS, (0, 0)
    )
    full_rows = lax.all_gather(tokens, "tp", axis=1, tiled=True)
    normed = rms_rows(full_rows, norm_gain)
    projected = jnp.dot(normed, in_whole, preferred_element_type=jnp.float32)
    pool_in = (projected * scale_in).astype(jnp.bfloat16)
    pooled = pool_local(pool_in, lax.axis_index("tp") * pool_in.shape[1])
    pooled_all = collect(pooled, "tp", 1)
    grouped = jnp.einsum(
        "lgc,gcd->lgd",
        pooled_all.reshape(length, 4, GROUP),
        pool_w,
        preferred_element_type=jnp.float32,
    )
    grouped = grouped.reshape(length, PW).astype(jnp.bfloat16)
    branch = jnp.dot(grouped, out_whole, preferred_element_type=jnp.float32)
    mixed = (tokens.astype(jnp.float32) + branch * scale_out).astype(jnp.bfloat16)
    mixed_full = lax.all_gather(mixed, "tp", axis=1, tiled=True)
    ffn_in = rms_rows(mixed_full, ffn_gain)
    upward = fold_rows(ffn_in, whole_of(w_up.astype(jnp.bfloat16), FS, (0, 1), 0))
    hidden = jnp.square(jax.nn.relu(upward * scale_up)).astype(jnp.bfloat16)
    partial_value = jnp.dot(
        hidden,
        whole_of(w_down.astype(jnp.bfloat16), FS, (0, 1), 1),
        preferred_element_type=jnp.float32,
    )
    rounded = lax.optimization_barrier((partial_value * scale_down).astype(jnp.bfloat16))
    summed = sent_and_summed(rounded.astype(jnp.float32).astype(jnp.bfloat16), "tp", 1)
    return (mixed.astype(jnp.float32) + summed).astype(jnp.bfloat16)[None]


def solution(mesh):
    finer = Mesh(
        mesh.devices.reshape(mesh.shape["rep"], 4, 4, mesh.shape["tp"]),
        ("rep", "fs_0", "fs_1", "tp"),
    )
    return jax.shard_map(
        on_device,
        mesh=finer,
        in_specs=(
            P(REP_FS, None, "tp"),
            P(),
            P(FS, "tp"),
            P(TP_FS),
            P(),
            P(FS, "tp"),
            P(TP_FS),
            P(),
            P(FS, "tp"),
            P(TP_FS),
            P("tp", FS),
            P(FS),
        ),
        out_specs=P(REP_FS, None, "tp"),
        check_vma=False,
    )
```

profile of v0, /device:TPU:1, one launch (start us, length us, event | category | flops | bytes accessed | tf_op | source)
XLA Modules:
  0.0 350.2 jit_solution(10267729505535979363)
XLA Ops:
  6.5 0.0 copy-start
  6.5 0.0 all-gather.18.cloned.1.call-start
  6.5 1.8 convert_element_type.116
  8.4 0.0 all-gather.18.cloned.1.call-update
  8.4 0.0 all-gather.22.cloned.1.call-start
  8.4 1.8 convert_element_type.118
  10.2 0.0 all-gather.22.cloned.1.call-update
  10.2 0.0 all-gather.16.cloned.1.call-start
  10.3 0.7 all-gather.16.cloned.1.call-update
  11.0 0.0 all-gather.20.cloned.1.call-start
  11.0 34.7 %all-gather.18.cloned.1.call-done = bf16[512,1024]{1,0:T(8,128)(2,1)} async-done(((bf16[128,1024]{1,0:T(8,128)(2,1)}), bf16[512,1024]{1,0:T(8,128)(2,1)}) %all-gather.18.cloned.1.call-update) | async-done | bytes 1048592 | tf_op jit(solution)/shard_map/all_gather | solution.py:45
  45.7 0.0 all-gather.20.cloned.1.call-update
  45.8 0.0 all-gather.24.cloned.1.call-start
  45.8 0.8 convert_element_type.100
  46.6 0.1 copy.25
  46.7 0.1 reshape.137
  46.8 0.8 convert_bitcast_fusion
  47.6 1.3 dynamic-slice
  49.6 0.9 maximum_dynamic-update-slice_fusion
  50.5 64.0 %all-reduce = f32[3392]{0:T(1024)S(1)} all-reduce(f32[3392]{0:T(1024)S(1)} %maximum_dynamic-update-slice_fusion), channel_id=4, replica_groups=mesh['rep'=2,'fs_0'=4,'fs_1'=4,'tp'=8] {'fs_0','fs_1'}, use_global_device_ids=true, to_apply=%add | all-reduce | flops 3392 | bytes 27136
  114.5 0.1 reshape.144
  114.6 0.1 mul.87
  114.7 33.1 %all-gather.1 = bf16[262144]{0:T(1024)(128)(2,1)S(1)} all-gather(bf16[16384]{0:T(1024)(128)(2,1)S(1)} %pad_maximum_fusion), channel_id=3, replica_groups=mesh['rep'=2,'fs_0'=4,'fs_1'=4,'tp'=8] {'fs_0','fs_1'}, dimensions={0}, use_global_device_ids=true | all-gather | bytes 557056 | tf_op jit(solution)/shard_map/all_gather | solution.py:23
  147.8 0.2 reshape.143
  148.1 0.0 all-gather.22.cloned.1.call-done
  148.1 0.0 all-gather.24.cloned.1.call-update
  148.2 0.5 reshape_reshape.12
  148.8 0.0 all-gather.16.cloned.1.call-done
  148.9 0.0 copy-start.1
  148.9 3.3 fusion.3
  152.2 0.2 copy-done.1
  152.4 1.5 fusion.69
  153.9 1.4 fusion.63
  155.3 1.4 fusion.57
  156.7 1.4 fusion.51
  158.1 0.0 copy-start.3
  158.1 1.4 fusion.72
  159.5 1.1 broadcast_in_dim.54
  160.6 26.7 %all-to-all-start = ((bf16[8,1024,64]{1,2,0:T(8,128)(2,1)}), bf16[8,1024,64]{1,2,0:T(8,128)(2,1)S(1)}, u32[]{:S(2)}, u32[]{:S(2)}) async-start(bf16[8,1024,64]{1,2,0:T(8,128)(2,1)} %broadcast_in_dim.54), calls=%async_computation | async-start | bytes 2097152 | tf_op jit(solution)/shard_map/all_to_all | solution.py:33
  187.3 0.0 all-gather.14.cloned.1.call-start
  187.3 0.1 slice.27
  187.4 0.1 mul.90
  187.5 0.1 reshape_reshape.14
  187.6 14.7 %all-to-all-done = bf16[8,1024,64]{1,2,0:T(8,128)(2,1)S(1)} async-done(((bf16[8,1024,64]{1,2,0:T(8,128)(2,1)}), bf16[8,1024,64]{1,2,0:T(8,128)(2,1)S(1)}, u32[]{:S(2)}, u32[]{:S(2)}) %all-to-all-start) | async-done | bytes 1048608 | tf_op jit(solution)/shard_map/all_to_all | solution.py:33
  202.3 0.0 copy-done
  202.3 0.5 convolution_convert_fusion
  202.8 1.3 fusion.38
  204.1 0.0 all-gather.14.cloned.1.call-update
  204.1 0.1 slice.28
  204.2 0.1 mul.98
  204.2 0.1 slice_bitcast_fusion
  204.3 4.8 %copy.28 = bf16[4,4,128,1024]{3,2,1,0:T(8,128)(2,1)} copy(bf16[4,4,128,1024]{3,2,0,1:T(8,128)(2,1)} %bitcast.61) | data formatting | bytes 8388608 | tf_op jit(solution)/shard_map/transpose | solution.py:48
  209.1 18.8 %all-gather.24.cloned.1.call-done = bf16[16,1024,128]{2,1,0:T(8,128)(2,1)} async-done(((bf16[4,1024,128]{2,1,0:T(8,128)(2,1)}), bf16[16,1024,128]{2,1,0:T(8,128)(2,1)}) %all-gather.24.cloned.1.call-update) | async-done | bytes 4194320 | tf_op jit(solution)/shard_map/all_gather | solution.py:45
  227.9 4.5 %copy.29 = bf16[4,4,1024,128]{3,2,1,0:T(8,128)(2,1)} copy(bf16[4,4,1024,128]{3,2,0,1:T(8,128)(2,1)} %bitcast.62) | data formatting | bytes 8388608 | tf_op jit(solution)/shard_map/transpose | solution.py:48
  232.4 6.4 %copy.30 = bf16[1024,16,128]{0,2,1:T(8,128)(2,1)} copy(bf16[1024,16,128]{2,0,1:T(8,128)(2,1)} %bitcast.59) | data formatting | bytes 8388608 | tf_op jit(solution)/shard_map/transpose | solution.py:16
  238.8 29.7 %all-gather.14.cloned.1.call-done = bf16[1024,2048]{1,0:T(8,128)(2,1)} async-done(((bf16[1024,256]{1,0:T(8,128)(2,1)}), bf16[1024,2048]{1,0:T(8,128)(2,1)}) %all-gather.14.cloned.1.call-update) | async-done | bytes 4194320 | tf_op jit(solution)/shard_map/all_gather | solution.py:122
  268.6 3.1 fusion
  271.6 0.0 copy-done.5
  271.6 14.6 %multiply_convert_fusion = bf16[1024,2048]{1,0:T(8,128)(2,1)} fusion(bf16[1024,2048]{0,1:T(8,128)(2,1)} %bitcast.64, f32[2048]{0:T(1024)S(1)} %slice_bitcast_fusion, f32[1024]{0:T(1024)S(1)} %mul.98, bf16[2048,1024]{1,0:T(8,128)(2,1)} %bitcast.63, bf16[1024,2048]{1,0:T(8,128)(2,1)} %all-gather.14.cloned.1.call-done, f32[2048]{0:T(1024)S(1)} %copy-done.5, ...), kind=kOutput, calls=%fused_computation.11 | convolution fusion | flops 8606711808 | bytes 16801792 | tf_op jit(solution)/shard_map/dot_general | solution.py:126
  286.3 2.5 copy.37
  288.7 52.6 %all_to_all.10 = bf16[8,1024,256]{2,1,0:T(8,128)(2,1)S(1)} all-to-all(bf16[8,1024,256]{2,1,0:T(8,128)(2,1)S(1)} %bitcast.60), channel_id=1, replica_groups=mesh['rep'=2,'fs_0'=4,'fs_1'=4,'tp'=8] {'tp'}, dimensions={0} | all-to-all | bytes 8388608 | tf_op jit(solution)/shard_map/all_to_all | solution.py:64
  341.4 0.6 convert_reduce_fusion
  342.0 0.5 copy-done.2
  342.4 0.9 fusion.79
  (23 shorter events, 0.2 us)
Async XLA Ops:
  6.5 195.7 %copy-start = (bf16[4,128,128]{2,1,0:T(8,128)(2,1)S(1)}, bf16[4,128,128]{2,1,0:T(8,128)(2,1)}, u32[]{:S(2)}) copy-start(bf16[4,128,128]{2,1,0:T(8,128)(2,1)} %param.16) | copy-start | bytes 393220
  6.5 39.2 %all-gather.18.cloned.1.call-start = ((), (), s32[]{:S(2)}) async-start(), calls=%async_computation.4 | async-start | bytes 1310720 | tf_op jit(solution)/shard_map/all_gather | solution.py:45
  8.4 139.7 %all-gather.22.cloned.1.call-start = ((), (), s32[]{:S(2)}) async-start(), calls=%async_computation.6 | async-start | bytes 1310720 | tf_op jit(solution)/shard_map/all_gather | solution.py:45
  10.2 138.6 %all-gather.16.cloned.1.call-start = ((), (), s32[]{:S(2)}) async-start(), calls=%async_computation.3 | async-start | bytes 4718592 | tf_op jit(solution)/shard_map/all_gather | solution.py:107
  11.0 193.4 %all-gather.20.cloned.1.call-start = ((), (), s32[]{:S(2)}) async-start(), calls=%async_computation.5 | async-start | bytes 5242880 | tf_op jit(solution)/shard_map/all_gather | solution.py:45
  45.8 182.1 %all-gather.24.cloned.1.call-start = ((), (), s32[]{:S(2)}) async-start(), calls=%async_computation.7 | async-start | bytes 5242880 | tf_op jit(solution)/shard_map/all_gather | solution.py:45
  147.8 4.3 %copy-start.4 = (f32[2048]{0:T(1024)S(1)}, f32[2048]{0:T(1024)}, u32[]{:S(2)}) copy-start(f32[2048]{0:T(1024)} %param.13) | copy-start | bytes 24580
  148.9 3.5 %copy-start.1 = (bf16[1,1024,2048]{2,1,0:T(8,128)(2,1)S(1)}, bf16[1,1024,2048]{2,1,0:T(8,128)(2,1)}, u32[]{:S(2)}) copy-start(bf16[1,1024,2048]{2,1,0:T(8,128)(2,1)} %all-gather.16.cloned.1.call-done) | copy-start | bytes 12582916
  158.1 44.7 %copy-start.3 = (bf16[1,1024,256]{2,1,0:T(8,128)(2,1)S(1)}, bf16[1,1024,256]{2,1,0:T(8,128)(2,1)}, u32[]{:S(2)}) copy-start(bf16[1,1024,256]{2,1,0:T(8,128)(2,1)} %param.12) | copy-start | bytes 1572868
  160.6 41.7 %all-to-all-start = ((bf16[8,1024,64]{1,2,0:T(8,128)(2,1)}), bf16[8,1024,64]{1,2,0:T(8,128)(2,1)S(1)}, u32[]{:S(2)}, u32[]{:S(2)}) async-start(bf16[8,1024,64]{1,2,0:T(8,128)(2,1)} %broadcast_in_dim.54), calls=%async_computation | async-start | bytes 2097152 | tf_op jit(solution)/shard_map/all_to_all | solution.py:33
  187.3 81.3 %all-gather.14.cloned.1.call-start = ((), (), s32[]{:S(2)}) async-start(), calls=%async_computation.2 | async-start | bytes 4718592 | tf_op jit(solution)/shard_map/all_gather | solution.py:122
  238.8 32.8 %copy-start.5 = (f32[2048]{0:T(1024)S(1)}, f32[2048]{0:T(1024)}, u32[]{:S(2)}) copy-start(f32[2048]{0:T(1024)} %param.19) | copy-start | bytes 24580
  341.4 1.0 copy-start.2
Sparse Core Ops, SparseCore 0:
  9.1 36.5 all-gather.17
  47.5 33.1 all-gather.21
  82.6 37.5 all-gather.15
  121.8 54.8 all-gather.19
  178.4 49.4 all-gather.23
  229.6 38.9 all-gather.13
where the time goes:
time: 351 us; the launch traced here: 350 us
  blocking collectives  150 us (43%)
  waiting for transfers between devices  98.7 us (28%)
  starting transfers between devices  26.9 us (8%)
  matrix products  23.5 us (7%)
  local copies, waits for them, and re-layouts  23.1 us (7%)
  between operations  14.4 us (4%)
  other arithmetic  13.9 us (4%)
    unnamed x1, blocking collectives  64 us
    all_gather x4, waiting for transfers between devices, stacked_from(): parts = lax.all_gather(parts, axes[k])  53.5 us
    all_to_all x1, blocking collectives, sent_and_summed(): parts = lax.all_to_all(cut_along(array, dim, count), axis, 0, 0, tiled=True)  52.6 us
    all_gather x1, blocking collectives, gather_packed(): lines, at, finished = (lax.all_gather(ravelled, axis), 0, [])  33.1 us
    all_gather x1, waiting for transfers between devices, on_device(): mixed_full = lax.all_gather(mixed, 'tp', axis=1, tiled=True)  29.7 us
    all_to_all x1, starting transfers between devices, sent_to_all(): lax.all_to_all(jnp.broadcast_to(array[None], (count, *array.shape)), axis...  26.7 us
    all_to_all x1, waiting for transfers between devices, sent_to_all(): lax.all_to_all(jnp.broadcast_to(array[None], (count, *array.shape)), axis...  14.7 us
    dot_general x1, matrix products, on_device(): jnp.dot(hidden, whole_of(w_down.astype(jnp.bfloat16), FS, (0, 1), 1), pre...  14.6 us
  transfers between devices with their start and end apart: 7, of which 4 were waited for; matrix products, arithmetic and copies ran while one was open for 10% of the time, Pallas kernels for 0%

commit v1 on v0

--- a/solution.py
+++ b/solution.py
@@ -10,6 +10,28 @@
 REP_FS = ("rep", "fs_0", "fs_1")
 TP_FS = ("tp", "fs_0", "fs_1")
 epsilon = 0.25
+
+
+def in_order(blocks, dim):
+    dims = list(blocks.shape[1:])
+    dims[dim] *= blocks.shape[0]
+    return jnp.moveaxis(blocks, 0, dim).reshape(dims)
+
+
+def doubled(shard, axis):
+    size = lax.axis_size(axis)
+    blocks = shard[None]
+    for level in range(size.bit_length() - 1):
+        bit = 1 << level
+        other = lax.ppermute(blocks, axis, [(i, i ^ bit) for i in range(size)])
+        both = jnp.stack([blocks, other])
+        upper = lax.axis_index(axis) >> level & 1
+        blocks = jnp.where(upper == 0, both, both[::-1]).reshape(-1, *shard.shape)
+    return blocks
+
+
+def gather_by_bits(value, axis, dim):
+    return in_order(doubled(value, axis), dim)
 
 
 def laid_out(parts, dim):
@@ -119,7 +141,7 @@
     grouped = grouped.reshape(length, PW).astype(jnp.bfloat16)
     branch = jnp.dot(grouped, out_whole, preferred_element_type=jnp.float32)
     mixed = (tokens.astype(jnp.float32) + branch * scale_out).astype(jnp.bfloat16)
-    mixed_full = lax.all_gather(mixed, "tp", axis=1, tiled=True)
+    mixed_full = gather_by_bits(mixed, "tp", 1)
     ffn_in = rms_rows(mixed_full, ffn_gain)
     upward = fold_rows(ffn_in, whole_of(w_up.astype(jnp.bfloat16), FS, (0, 1), 0))
     hidden = jnp.square(jax.nn.relu(upward * scale_up)).astype(jnp.bfloat16)

time: 351 us -> 369 us (1.051)
  waiting for transfers between devices: 98.7 us -> 106 us
  other arithmetic: 13.9 us -> 20 us
    ppermute x0 -> x3, waiting for transfers between devices: none -> 56.4 us  [doubled(): other = lax.ppermute(blocks, axis, [(i, i ^ bit) for i in range(size)])]
    all_gather x1 -> x0, waiting for transfers between devices: 29.7 us -> none  [on_device(): mixed_full = lax.all_gather(mixed, 'tp', axis=1, tiled=True)]
    all_gather x4, waiting for transfers between devices: 53.5 us -> 34.7 us  [stacked_from(): parts = lax.all_gather(parts, axes[k])]
    another operation x0 -> x4, other arithmetic: none -> 3.91 us  [doubled(): both = jnp.stack([blocks, other])]
  transfers between devices with their start and end apart: 7 -> 9, of which waited for: 4 -> 5; matrix products, arithmetic and copies ran while one was open for 10% -> 11% of each run, Pallas kernels for 0% -> 0%
where the time goes in v1:
time: 369 us; the launch traced here: 368 us
  blocking collectives  151 us (41%)
  waiting for transfers between devices  106 us (29%)
  starting transfers between devices  29.4 us (8%)
  local copies, waits for them, and re-layouts  24.7 us (7%)
  matrix products  23.1 us (6%)
  other arithmetic  20 us (5%)
  between operations  14.1 us (4%)
    unnamed x1, blocking collectives  63.9 us
    ppermute x3, waiting for transfers between devices, doubled(): other = lax.ppermute(blocks, axis, [(i, i ^ bit) for i in range(size)])  56.4 us
    all_to_all x1, blocking collectives, sent_and_summed(): parts = lax.all_to_all(cut_along(array, dim, count), axis, 0, 0, tiled=True)  53.3 us
    all_gather x4, waiting for transfers between devices, stacked_from(): parts = lax.all_gather(parts, axes[k])  34.7 us
    all_gather x1, blocking collectives, gather_packed(): lines, at, finished = (lax.all_gather(ravelled, axis), 0, [])  33.7 us
    all_to_all x1, starting transfers between devices, sent_to_all(): lax.all_to_all(jnp.broadcast_to(array[None], (count, *array.shape)), axis...  26.7 us
    dot_general x1, matrix products, on_device(): jnp.dot(hidden, whole_of(w_down.astype(jnp.bfloat16), FS, (0, 1), 1), pre...  14.4 us
    all_to_all x1, waiting for transfers between devices, sent_to_all(): lax.all_to_all(jnp.broadcast_to(array[None], (count, *array.shape)), axis...  13.9 us
  transfers between devices with their start and end apart: 9, of which 5 were waited for; matrix products, arithmetic and copies ran while one was open for 11% of the time, Pallas kernels for 0%

profile of v1, /device:TPU:1, one launch (start us, length us, event | category | flops | bytes accessed | tf_op | source)
XLA Modules:
  0.0 368.2 jit_solution(15633538210918152489)
XLA Ops:
  6.5 1.8 convert_element_type.133
  8.4 0.0 all-gather.15.cloned.1.call-start
  8.4 1.8 convert_element_type.131
  10.3 0.0 all-gather.13.cloned.1.call-start
  10.3 0.7 all-gather.13.cloned.1.call-update
  11.0 0.0 all-gather.21.cloned.1.call-start
  11.0 34.7 %all-gather.19.cloned.1.call-done = bf16[4096,128]{1,0:T(8,128)(2,1)} async-done(((bf16[1024,128]{1,0:T(8,128)(2,1)}), bf16[4096,128]{1,0:T(8,128)(2,1)}) %all-gather.19.cloned.1.call-update) | async-done | bytes 1048592 | tf_op jit(solution)/shard_map/all_gather | solution.py:67
  45.8 0.0 all-gather.17.cloned.1.call-start
  45.8 1.3 dynamic-slice
  47.8 0.9 maximum_dynamic-update-slice_fusion
  48.7 63.9 %all-reduce = f32[3392]{0:T(1024)S(1)} all-reduce(f32[3392]{0:T(1024)S(1)} %maximum_dynamic-update-slice_fusion), channel_id=4, replica_groups=mesh['rep'=2,'fs_0'=4,'fs_1'=4,'tp'=8] {'fs_0','fs_1'}, use_global_device_ids=true, to_apply=%add | all-reduce | flops 3392 | bytes 27136
  112.6 0.1 reshape.168
  112.7 0.1 mul.95
  112.8 0.8 convert_element_type.112
  113.6 0.1 copy.32
  113.7 0.1 reshape.158
  113.8 0.8 convert_bitcast_fusion
  114.6 33.7 %all-gather.1 = bf16[262144]{0:T(1024)(128)(2,1)S(1)} all-gather(bf16[16384]{0:T(1024)(128)(2,1)S(1)} %pad_maximum_fusion.3), channel_id=3, replica_groups=mesh['rep'=2,'fs_0'=4,'fs_1'=4,'tp'=8] {'fs_0','fs_1'}, dimensions={0}, use_global_device_ids=true | all-gather | bytes 557056 | tf_op jit(solution)/shard_map/all_gather | solution.py:45
  148.3 0.2 reshape.167
  148.6 0.5 reshape_reshape.12
  149.2 0.0 all-gather.15.cloned.1.call-done
  149.3 3.3 fusion
  152.7 0.2 copy-done.2
  152.9 1.5 fusion.63
  154.3 1.4 fusion.57
  155.7 1.4 fusion.51
  157.1 1.4 fusion.45
  158.5 1.4 fusion.66
  159.9 1.2 broadcast_in_dim.57
  161.1 26.7 %all-to-all-start = ((bf16[8,1024,64]{1,2,0:T(8,128)(2,1)}), bf16[8,1024,64]{1,2,0:T(8,128)(2,1)S(1)}, u32[]{:S(2)}, u32[]{:S(2)}) async-start(bf16[8,1024,64]{1,2,0:T(8,128)(2,1)} %broadcast_in_dim.57), calls=%async_computation | async-start | bytes 2097152 | tf_op jit(solution)/shard_map/all_to_all | solution.py:55
  187.8 0.1 slice.27
  187.9 0.2 copy.31
  188.1 0.6 mul.98
  188.8 0.1 reshape_reshape.14
  188.9 13.9 %all-to-all-done = bf16[8,1024,64]{1,2,0:T(8,128)(2,1)S(1)} async-done(((bf16[8,1024,64]{1,2,0:T(8,128)(2,1)}), bf16[8,1024,64]{1,2,0:T(8,128)(2,1)S(1)}, u32[]{:S(2)}, u32[]{:S(2)}) %all-to-all-start) | async-done | bytes 1048608 | tf_op jit(solution)/shard_map/all_to_all | solution.py:55
  202.8 0.5 convolution_convert_fusion
  203.3 1.2 fusion.32
  204.5 1.1 collective-permute-start
  205.5 1.5 collective-permute-done
  207.1 0.1 pad_maximum_fusion.2
  207.2 0.4 fusion.70
  207.6 0.5 collective-permute-start.1
  208.1 24.2 %collective-permute-done.1 = bf16[2,1024,256]{1,2,0:T(8,128)(2,1)} collective-permute-done((bf16[2,1024,256]{1,2,0:T(8,128)(2,1)S(1)}, bf16[2,1024,256]{1,2,0:T(8,128)(2,1)}, u32[]{:S(2)}, u32[]{:S(2)}) %collective-permute-start.1) | collective-permute-done | bytes 1048608 | tf_op jit(solution)/shard_map/ppermute | solution.py:26
  232.3 1.4 pad_maximum_fusion.1
  233.7 0.6 reverse_select_fusion.1
  234.3 1.0 collective-permute-start.2
  235.3 0.1 slice.28
  235.4 0.1 mul.107
  235.4 0.1 slice_bitcast_fusion
  235.5 4.6 %copy.36 = bf16[4,4,1024,128]{3,2,1,0:T(8,128)(2,1)} copy(bf16[4,4,1024,128]{3,2,0,1:T(8,128)(2,1)} %bitcast.82) | data formatting | bytes 8388608 | tf_op jit(solution)/shard_map/transpose | solution.py:70
  240.1 6.5 %copy.37 = bf16[1024,16,128]{0,2,1:T(8,128)(2,1)} copy(bf16[1024,16,128]{2,0,1:T(8,128)(2,1)} %bitcast.78) | data formatting | bytes 8388608 | tf_op jit(solution)/shard_map/transpose | solution.py:38
  246.5 4.8 %copy.35 = bf16[4,4,128,1024]{3,2,1,0:T(8,128)(2,1)} copy(bf16[4,4,128,1024]{3,2,0,1:T(8,128)(2,1)} %bitcast.83) | data formatting | bytes 8388608 | tf_op jit(solution)/shard_map/transpose | solution.py:70
  251.3 30.7 %collective-permute-done.2 = bf16[4,1024,256]{1,2,0:T(8,128)(2,1)} collective-permute-done((bf16[4,1024,256]{1,2,0:T(8,128)(2,1)S(1)}, bf16[4,1024,256]{1,2,0:T(8,128)(2,1)}, u32[]{:S(2)}, u32[]{:S(2)}) %collective-permute-start.2) | collective-permute-done | bytes 2097184 | tf_op jit(solution)/shard_map/ppermute | solution.py:26
  282.0 2.0 pad_maximum_fusion
  283.9 1.4 reverse_select_fusion
  285.4 1.2 fusion.3
  286.6 2.8 fusion.5
  289.4 14.4 %multiply_convert_fusion = bf16[1024,2048]{1,0:T(8,128)(2,1)} fusion(bf16[1024,2048]{0,1:T(8,128)(2,1)} %bitcast.84, f32[2048]{0:T(1024)S(1)} %slice_bitcast_fusion, bf16[1024,2048]{0,1:T(8,128)(2,1)} %bitcast.86, bf16[2048,1024]{1,0:T(8,128)(2,1)} %bitcast.85, f32[1024]{0:T(1024)S(1)} %mul.107), kind=kOutput, calls=%fused_computation.11 | convolution fusion | flops 8598323200 | bytes 16789504 | tf_op jit(solution)/shard_map/dot_general | solution.py:148
  303.8 2.5 copy.48
  306.2 53.3 %all_to_all.10 = bf16[8,1024,256]{2,1,0:T(8,128)(2,1)S(1)} all-to-all(bf16[8,1024,256]{2,1,0:T(8,128)(2,1)S(1)} %bitcast.79), channel_id=1, replica_groups=mesh['rep'=2,'fs_0'=4,'fs_1'=4,'tp'=8] {'tp'}, dimensions={0} | all-to-all | bytes 8388608 | tf_op jit(solution)/shard_map/all_to_all | solution.py:86
  359.6 0.6 convert_reduce_fusion
  360.2 0.3 copy.40
  360.5 0.1 fusion.71
  360.6 1.0 copy.41
  (37 shorter events, 0.3 us)
Async XLA Ops:
  6.5 196.3 %copy-start = (bf16[4,128,128]{2,1,0:T(8,128)(2,1)S(1)}, bf16[4,128,128]{2,1,0:T(8,128)(2,1)}, u32[]{:S(2)}) copy-start(bf16[4,128,128]{2,1,0:T(8,128)(2,1)} %param.16) | copy-start | bytes 393220
  6.5 39.2 %all-gather.19.cloned.1.call-start = ((), (), s32[]{:S(2)}) async-start(), calls=%async_computation.5 | async-start | bytes 1310720 | tf_op jit(solution)/shard_map/all_gather | solution.py:67
  8.4 140.9 %all-gather.15.cloned.1.call-start = ((), (), s32[]{:S(2)}) async-start(), calls=%async_computation.3 | async-start | bytes 1310720 | tf_op jit(solution)/shard_map/all_gather | solution.py:67
  10.3 139.1 %all-gather.13.cloned.1.call-start = ((), (), s32[]{:S(2)}) async-start(), calls=%async_computation.2 | async-start | bytes 4718592 | tf_op jit(solution)/shard_map/all_gather | solution.py:129
  11.0 224.5 %all-gather.21.cloned.1.call-start = ((), (), s32[]{:S(2)}) async-start(), calls=%async_computation.6 | async-start | bytes 5242880 | tf_op jit(solution)/shard_map/all_gather | solution.py:67
  45.8 200.8 %all-gather.17.cloned.1.call-start = ((), (), s32[]{:S(2)}) async-start(), calls=%async_computation.4 | async-start | bytes 5242880 | tf_op jit(solution)/shard_map/all_gather | solution.py:67
  148.3 4.4 %copy-start.5 = (f32[2048]{0:T(1024)S(1)}, f32[2048]{0:T(1024)}, u32[]{:S(2)}) copy-start(f32[2048]{0:T(1024)} %param.13) | copy-start | bytes 24580
  149.3 3.5 copy-start.2
  158.5 29.4 %copy-start.3 = (bf16[1,1024,256]{2,1,0:T(8,128)(2,1)S(1)}, bf16[1,1024,256]{2,1,0:T(8,128)(2,1)}, u32[]{:S(2)}) copy-start(bf16[1,1024,256]{2,1,0:T(8,128)(2,1)} %param.12) | copy-start | bytes 1572868
  161.1 41.7 %all-to-all-start = ((bf16[8,1024,64]{1,2,0:T(8,128)(2,1)}), bf16[8,1024,64]{1,2,0:T(8,128)(2,1)S(1)}, u32[]{:S(2)}, u32[]{:S(2)}) async-start(bf16[8,1024,64]{1,2,0:T(8,128)(2,1)} %broadcast_in_dim.57), calls=%async_computation | async-start | bytes 2097152 | tf_op jit(solution)/shard_map/all_to_all | solution.py:55
  204.5 2.6 collective-permute-start
  207.6 24.7 %collective-permute-start.1 = (bf16[2,1024,256]{1,2,0:T(8,128)(2,1)S(1)}, bf16[2,1024,256]{1,2,0:T(8,128)(2,1)}, u32[]{:S(2)}, u32[]{:S(2)}) collective-permute-start(bf16[2,1024,256]{1,2,0:T(8,128)(2,1)S(1)} %get-tuple-element.6), channel_id=1, source_target_pairs={{0,2},{1,3},{2,0},{3,1},{4,6},{5,7},{6,4},{7,5},{8,10},{9,11},{10,... | collective-permute-start | bytes 3145736 | tf_op jit(solution)/shard_map/ppermute | solution.py:26
  232.3 3.1 copy-start.4
  234.3 47.7 %collective-permute-start.2 = (bf16[4,1024,256]{1,2,0:T(8,128)(2,1)S(1)}, bf16[4,1024,256]{1,2,0:T(8,128)(2,1)}, u32[]{:S(2)}, u32[]{:S(2)}) collective-permute-start(bf16[4,1024,256]{1,2,0:T(8,128)(2,1)S(1)} %bitcast.80), channel_id=1, source_target_pairs={{0,4},{1,5},{2,6},{3,7},{4,0},{5,1},{6,2},{7,3},{8,12},{9,13},{10,... | collective-permute-start | bytes 6291464 | tf_op jit(solution)/shard_map/ppermute | solution.py:26
  306.2 55.4 %copy-start.1 = (bf16[4,128,128]{2,1,0:T(8,128)(2,1)S(1)}, bf16[4,128,128]{2,1,0:T(8,128)(2,1)}, u32[]{:S(2)}) copy-start(bf16[4,128,128]{2,1,0:T(8,128)(2,1)} %param.16) | copy-start | bytes 393220
Sparse Core Ops, SparseCore 0:
  9.1 36.5 all-gather.18
  47.5 33.1 all-gather.14
  82.6 37.4 all-gather.12
  121.8 54.6 all-gather.20
  178.2 49.5 all-gather.16
